TPU v7x, 256 devices: a 4x2x16 block of a 4x16x16 slice. The times are simulated.
256 devices in a mesh: grp: 2 (over y), sp: 16 (over z), tp: 8 (over x, core).
Axes of the slice: x: 4, y: 2, z: 16, core: 2. Of those that a mesh axis runs over, the one named last changes fastest.
The devices are a block of a 4x16x16 slice.
Arguments:
- queries: bfloat16 [24576, 1024], P(('grp', 'sp'), 'tp'), parts along dimension 0, may hold values from -8 to 8
- keys: bfloat16 [24576, 256], P(('grp', 'sp')), parts along dimension 0, may hold values from -8 to 8
- values: bfloat16 [24576, 256], P(('grp', 'sp')), parts along dimension 0, may hold values from -6 to 6
- query_gain: float32 [128], replicated, may hold values from 0.2 to 6
- key_gain: float32 [128], replicated, may hold values from 0.2 to 6
- residual: bfloat16 [24576, 2048], P(('grp', 'sp', 'tp')), parts along dimension 0, may hold values from -6 to 6
- out_weight: bfloat16 [1024, 2048], P('tp'), may hold values from -0.1875 to 0.1875
- mix_gain: float32 [2048], replicated, may hold values from 0.1 to 1.9
- ffn_gain: float32 [2048], replicated, may hold values from 0.1 to 1.9
- gate_in: bfloat16 [2048, 5632], P('sp', 'tp'), may hold values from -0.125 to 0.125
- value_in: bfloat16 [2048, 5632], P('sp', 'tp'), may hold values from -0.125 to 0.125
- conv_gate: float32 [3, 5632], P(None, 'tp'), may hold values from -3 to 3
- conv_value: float32 [3, 5632], P(None, 'tp'), may hold values from -3 to 3
- down_t: bfloat16 [2048, 5632], P('sp', 'tp'), may hold values from -0.078125 to 0.078125
Outputs:
- layer_out: bfloat16 [24576, 2048], P(('grp', 'sp', 'tp')), parts along dimension 0
There are 2 independent parts, one for each index of `grp`. A program takes and returns all parts, laid end to end along the dimension named above; an argument that names none is the same for every part. Nothing has to cross between parts.
All inputs are finite; a program needn't handle non-finite values.
Results may differ from a plain program's by a relative error of at most 0.02.
The roundings to bfloat16 on the way count: a program that leaves them out, or rounds other values in their place, can miss the bound.
Values may be sent and summed in bfloat16 or wider, within the bound.
A program may use at most 128 MiB of HBM per device.

v0:
```python
import jax
import jax.numpy as jnp
from jax import lax
from jax.sharding import PartitionSpec as P

HEADS = 8
KVH = 2
GRID_W = 64
EPSILON = 1e-06
THETA = 10000.0


def sent_together(arrays, axis, dim, along):
    both = jnp.concatenate(arrays, axis=along)
    whole, at, gathered = (lax.all_gather(both, axis, axis=dim, tiled=True), 0, [])
    for a in arrays:
        gathered.append(lax.slice_in_dim(whole, at, at + a.shape[along], axis=along))
        at += a.shape[along]
    return tuple(gathered)


def cut_along(array, dim, size):
    before, after = (array.shape[:dim], array.shape[dim + 1 :])
    return jnp.moveaxis(array.reshape(*before, size, -1, *after), dim, 0)


def summed_on_arrival(array, axis, dim):
    tiles = cut_along(array, dim, lax.axis_size(axis))
    arrived = lax.all_to_all(tiles, axis, split_axis=0, concat_axis=0, tiled=True)
    return arrived.astype(jnp.float32).sum(axis=0)


def with_halo(block, sides, width):
    for axis, dim in sides:
        count = lax.axis_size(axis)
        forward = [(i, i + 1) for i in range(count - 1)]
        backward = [(target, source) for source, target in forward]
        low = lax.ppermute(
            lax.slice_in_dim(block, block.shape[dim] - width, None, axis=dim), axis, forward
        )
        high = lax.ppermute(lax.slice_in_dim(block, 0, width, axis=dim), axis, backward)
        block = jnp.concatenate([low, block, high], axis=dim)
    return block


def rotary_tables(positions, seq_total, head_dim):
    quarter = head_dim // 4
    inverse = THETA ** (-(2.0 * jnp.arange(quarter, dtype=jnp.float32)) / (head_dim // 2))
    grid_row = (positions // GRID_W - seq_total // GRID_W // 2).astype(jnp.float32)
    grid_col = (positions % GRID_W - GRID_W // 2).astype(jnp.float32)
    row_angle = grid_row[:, None] * inverse[None, :]
    col_angle = grid_col[:, None] * inverse[None, :]
    angle = jnp.concatenate([row_angle, row_angle, col_angle, col_angle], axis=-1)
    return (jnp.cos(angle), jnp.sin(angle))


def rotate_quarters(vector):
    first, second, third, fourth = jnp.split(vector, 4, axis=-1)
    return jnp.concatenate([-second, first, -fourth, third], axis=-1)


def prepare_heads(raw, gain, cos_table, sin_table, factor):
    floats = raw.astype(jnp.float32)
    normed = floats * lax.rsqrt(jnp.mean(floats * floats, axis=-1, keepdims=True) + EPSILON) * gain
    turned = normed * cos_table + rotate_quarters(normed) * sin_table
    return (turned * factor).astype(jnp.bfloat16)


def rms_rows(stream, gain):
    floats = stream.astype(jnp.float32)
    return floats * lax.rsqrt(jnp.mean(floats * floats, axis=-1, keepdims=True) + EPSILON) * gain


def body(
    queries,
    keys,
    values,
    query_gain,
    key_gain,
    residual,
    out_weight,
    mix_gain,
    ffn_gain,
    gate_in,
    value_in,
    conv_gate,
    conv_value,
    down_t,
):
    gate_rows, value_rows, down_rows = sent_together((gate_in, value_in, down_t), "sp", 0, 1)
    tok_rows = queries.shape[0]
    head_dim = query_gain.shape[0]
    local_heads = queries.shape[1] // head_dim
    seq_total = tok_rows * lax.axis_size("sp")
    kv_head = lax.axis_index("tp") * local_heads // (HEADS // KVH)
    positions = lax.axis_index("sp") * tok_rows + jnp.arange(tok_rows, dtype=jnp.int32)
    cos_table, sin_table = rotary_tables(positions, seq_total, head_dim)
    key_own = lax.dynamic_slice_in_dim(keys, kv_head * head_dim, head_dim, 1)
    value_own = lax.dynamic_slice_in_dim(values, kv_head * head_dim, head_dim, 1)
    key_rot = prepare_heads(key_own, key_gain, cos_table, sin_table, 1.0)
    query_rot = prepare_heads(
        queries.reshape(tok_rows, local_heads, head_dim),
        query_gain,
        cos_table[:, None, :],
        sin_table[:, None, :],
        head_dim ** (-0.5),
    )
    query_rows = jnp.transpose(query_rot, (1, 0, 2)).reshape(local_heads * tok_rows, head_dim)
    query_count = local_heads * tok_rows
    running = jnp.full((query_count, 1), -1e30, jnp.float32)
    key_piece, value_piece = sent_together((key_rot, value_own), "sp", 0, 1)
    scores = lax.dot_general(
        query_rows, key_piece, (((1,), (1,)), ((), ())), preferred_element_type=jnp.float32
    )
    newest = jnp.maximum(running, jnp.max(scores, axis=1, keepdims=True))
    weights = jnp.exp(scores - newest)
    denom = jnp.sum(weights, axis=1, keepdims=True)
    summed = jnp.dot(weights.astype(jnp.bfloat16), value_piece, preferred_element_type=jnp.float32)
    running, denom, summed = (newest, denom, summed)
    attended = (summed / denom).astype(jnp.bfloat16).reshape(local_heads, tok_rows, head_dim)
    attended = jnp.transpose(attended, (1, 0, 2)).reshape(tok_rows, local_heads * head_dim)
    block_rows = attended
    mix = summed_on_arrival(
        jnp.dot(block_rows, out_weight, preferred_element_type=jnp.float32).astype(jnp.bfloat16),
        "tp",
        0,
    )
    stream = (residual.astype(jnp.float32) + rms_rows(mix, mix_gain)).astype(jnp.bfloat16)
    normed = rms_rows(stream, ffn_gain).astype(jnp.bfloat16)
    paired = jnp.concatenate([gate_rows, value_rows], axis=1)
    upward = jnp.dot(
        lax.all_gather(normed, "tp", axis=0, tiled=True), paired, preferred_element_type=jnp.float32
    ).astype(jnp.bfloat16)
    padded = with_halo(upward, (("sp", 0),), 1).astype(jnp.float32)
    taps = jnp.concatenate([conv_gate, conv_value], axis=1)
    mixed = taps[0] * padded[:-2] + taps[1] * padded[1:-1] + taps[2] * padded[2:]
    unit_cols = conv_gate.shape[1]
    hidden = (jax.nn.gelu(mixed[:, :unit_cols], approximate=True) * mixed[:, unit_cols:]).astype(
        jnp.bfloat16
    )
    block_rows = hidden
    ffn_out = summed_on_arrival(
        lax.dot_general(
            block_rows, down_rows, (((1,), (1,)), ((), ())), preferred_element_type=jnp.float32
        ).astype(jnp.bfloat16),
        "tp",
        0,
    )
    return (stream.astype(jnp.float32) + ffn_out).astype(jnp.bfloat16)


def solution(mesh):
    return jax.shard_map(
        body,
        mesh=mesh,
        in_specs=(
            P(("grp", "sp"), "tp"),
            P(("grp", "sp"), None),
            P(("grp", "sp"), None),
            P(),
            P(),
            P(("grp", "sp", "tp"), None),
            P("tp", None),
            P(),
            P(),
            P("sp", "tp"),
            P("sp", "tp"),
            P(None, "tp"),
            P(None, "tp"),
            P("sp", "tp"),
        ),
        out_specs=P(("grp", "sp", "tp"), None),
        check_vma=False,
    )
```

profile of v0, /device:TPU:33, one launch (start us, length us, event | category | flops | bytes accessed | tf_op | source)
XLA Modules:
  0.0 345.3 jit_solution(11012669087130800998)
XLA Ops:
  6.5 0.0 copy-start
  6.6 0.0 copy-start.3
  6.6 0.0 copy-start.10
  6.6 0.0 all-gather.4.cloned.1.call-start
  6.6 1.2 fusion.55
  7.8 1.1 fusion.56
  8.9 0.0 copy-start.2
  8.9 0.0 copy-start.9
  8.9 0.4 slice_negate_fusion.1
  9.3 0.9 constant_dynamic-slice_fusion
  10.3 0.3 broadcast_multiply_fusion.1
  10.6 0.0 copy-done.3
  10.6 0.0 copy-done.10
  10.6 2.0 fusion.60
  12.6 0.8 pad_maximum_fusion.2
  13.4 0.1 all-gather.4.cloned.1.call-update
  13.4 0.1 all-gather.8.cloned.1.call-start
  13.5 1.9 pad_maximum_fusion
  15.4 0.1 all-gather.8.cloned.1.call-update
  15.5 0.1 all-gather.6.cloned.1.call-start
  15.6 0.0 copy-done.2
  15.6 0.2 fusion.48
  15.8 0.0 copy-done.9
  15.8 0.2 fusion.50
  16.0 0.4 fusion.58
  16.3 93.2 %all-gather.4.cloned.1.call-done = bf16[12288,256]{1,0:T(8,128)(2,1)} async-done(((bf16[768,256]{1,0:T(8,128)(2,1)}), bf16[12288,256]{1,0:T(8,128)(2,1)}) %all-gather.4.cloned.1.call-update) | async-done | bytes 6291472 | tf_op jit(solution)/shard_map/all_gather | solution.py:15
  109.5 16.3 %fusion.87 = (f32[768]{0:T(1024)S(1)}, f32[768,12288]{1,0:T(8,128)}) fusion(bf16[12288,256]{1,0:T(8,128)(2,1)} %all-gather.4.cloned.1.call-done, bf16[768,128]{1,0:T(8,128)(2,1)S(1)} %copy-done.2, f32[768,32]{1,0:T(8,128)S(1)} %get-tuple-element.13, f32[768,32]{1,0:T(8,128)S(1)} %get-tuple-element.14, f32[768,32]{1,0:T(8,128)S(1)} %get-tuple-element.15, ...), kind=kOutput, calls=%fused_computation.117 | convolution fusion | flops 2426731776 | bytes 41687552 | tf_op jit(solution)/shard_map/dot_general | solution.py:112
  125.9 15.4 %fusion = f32[768]{0:T(1024)S(1)} fusion(f32[768,12288]{1,0:T(8,128)} %get-tuple-element.23, f32[768]{0:T(1024)S(1)} %broadcast_maximum_fusion), kind=kLoop, calls=%fused_computation.1 | loop fusion | flops 18873600 | bytes 37754880 | tf_op jit(solution)/shard_map/reduce_sum | solution.py:117
  141.2 0.0 copy-done
  141.2 18.7 %convolution_convert_fusion.1 = bf16[768,2048]{1,0:T(8,128)(2,1)} fusion(bf16[128,2048]{1,0:T(8,128)(2,1)S(1)} %copy-done, bf16[12288,256]{1,0:T(8,128)(2,1)} %all-gather.4.cloned.1.call-done, f32[768,12288]{1,0:T(8,128)} %get-tuple-element.23, f32[768]{0:T(1024)S(1)} %broadcast_maximum_fusion, f32[768]{0:T(1024)S(1)} %fusion), kind=kOutput, calls=%fused_computation.16 | convolution fusion | flops 2839216128 | bytes 44570624 | tf_op jit(solution)/shard_map/dot_general | solution.py:124
  159.9 0.0 copy-start.4
  159.9 0.0 copy-start.7
  159.9 45.7 %all_to_all.10 = bf16[8,96,2048]{2,1,0:T(8,128)(2,1)S(1)} all-to-all(bf16[8,96,2048]{2,1,0:T(8,128)(2,1)} %bitcast.14), channel_id=1, replica_groups=mesh['grp'=2,'sp'=16,'tp'=8] {'tp'}, dimensions={0} | all-to-all | bytes 6291456 | tf_op jit(solution)/shard_map/all_to_all | solution.py:29
  205.6 0.0 copy-start.8
  205.6 0.6 convert_reduce_fusion.1
  206.2 0.1 multiply_reduce_fusion
  206.3 0.0 copy-done.4
  206.3 0.0 copy-done.7
  206.3 0.3 fusion.44
  206.7 0.0 copy-done.8
  206.7 0.9 fusion.46
  207.6 0.1 all-gather.6.cloned.1.call-update
  207.7 0.0 copy-start.5
  207.7 0.0 copy-start.6
  207.7 22.5 %all-gather.8.cloned.1.call-done = bf16[2048,2112]{0,1:T(8,128)(2,1)} async-done(((bf16[128,2112]{0,1:T(8,128)(2,1)}), bf16[2048,2112]{0,1:T(8,128)(2,1)}) %all-gather.8.cloned.1.call-update) | async-done | bytes 8650768 | tf_op jit(solution)/shard_map/all_gather | solution.py:15
  230.2 42.3 %all-gather.6.cloned.1.call-done = bf16[768,2048]{1,0:T(8,128)(2,1)} async-done(((bf16[96,2048]{1,0:T(8,128)(2,1)}), bf16[768,2048]{1,0:T(8,128)(2,1)}) %all-gather.6.cloned.1.call-update) | async-done | bytes 3145744 | tf_op jit(solution)/shard_map/all_gather | solution.py:132
  272.5 8.4 %fusion.9 = bf16[768,1408]{1,0:T(8,128)(2,1)S(1)} fusion(bf16[768,2048]{1,0:T(8,128)(2,1)} %all-gather.6.cloned.1.call-done, bf16[2048,2112]{0,1:T(8,128)(2,1)} %all-gather.8.cloned.1.call-done), kind=kOutput, calls=%fused_computation.17 | convolution fusion | flops 4430266368 | bytes 11075584 | tf_op jit(solution)/shard_map/dot_general | solution.py:131
  280.9 3.2 collective-permute-start
  284.1 1.3 collective-permute-start.1
  285.4 0.0 copy-done.5
  285.4 0.0 copy-done.6
  285.4 0.1 maximum_reduce_fusion.1
  285.5 0.0 collective-permute-done
  285.6 2.9 collective-permute-done.1
  288.5 0.4 maximum_convert_fusion
  288.9 1.3 fusion.7
  290.2 5.1 %convolution_convert_fusion = bf16[768,2048]{1,0:T(8,128)(2,1)S(1)} fusion(bf16[2048,2112]{0,1:T(8,128)(2,1)} %all-gather.8.cloned.1.call-done, f32[768,1408]{1,0:T(8,128)S(1)} %fusion.7), kind=kOutput, calls=%fused_computation.15 | convolution fusion | flops 2221572096 | bytes 10747904 | tf_op jit(solution)/shard_map/dot_general | solution.py:143
  295.3 0.0 copy-start.1
  295.3 42.0 %all_to_all.11 = bf16[8,96,2048]{2,1,0:T(8,128)(2,1)S(1)} all-to-all(bf16[8,96,2048]{2,1,0:T(8,128)(2,1)S(1)} %bitcast.15), channel_id=1, replica_groups=mesh['grp'=2,'sp'=16,'tp'=8] {'tp'}, dimensions={0} | all-to-all | bytes 6291456 | tf_op jit(solution)/shard_map/all_to_all | solution.py:29
  337.3 0.6 convert_reduce_fusion
  337.9 0.8 fusion.47
  338.7 0.0 copy-done.1
  (8 shorter events, 0.1 us)
Async XLA Ops:
  6.5 134.7 %copy-start = (bf16[128,2048]{1,0:T(8,128)(2,1)S(1)}, bf16[128,2048]{1,0:T(8,128)(2,1)}, u32[]{:S(2)}) copy-start(bf16[128,2048]{1,0:T(8,128)(2,1)} %param.20) | copy-start | bytes 1572868
  6.6 4.0 %copy-start.3 = (bf16[768,256]{1,0:T(8,128)(2,1)S(1)}, bf16[768,256]{1,0:T(8,128)(2,1)}, u32[]{:S(2)}) copy-start(bf16[768,256]{1,0:T(8,128)(2,1)} %param.15) | copy-start | bytes 1179652
  6.6 4.0 %copy-start.10 = (f32[128]{0:T(128)S(1)}, f32[128]{0:T(128)}, u32[]{:S(2)}) copy-start(f32[128]{0:T(128)} %param.18) | copy-start | bytes 1540
  6.6 103.0 %all-gather.4.cloned.1.call-start = ((), (), s32[]{:S(2)}) async-start(), calls=%async_computation.2 | async-start | bytes 6684672 | tf_op jit(solution)/shard_map/all_gather | solution.py:15
  8.9 6.6 %copy-start.2 = (bf16[768,128]{1,0:T(8,128)(2,1)S(1)}, bf16[768,128]{1,0:T(8,128)(2,1)}, u32[]{:S(2)}) copy-start(bf16[768,128]{1,0:T(8,128)(2,1)} %param.14) | copy-start | bytes 589828
  8.9 6.8 %copy-start.9 = (f32[128]{0:T(128)S(1)}, f32[128]{0:T(128)}, u32[]{:S(2)}) copy-start(f32[128]{0:T(128)} %param.17) | copy-start | bytes 1540
  13.4 216.8 %all-gather.8.cloned.1.call-start = ((), (), s32[]{:S(2)}) async-start(), calls=%async_computation.4 | async-start | bytes 9191424 | tf_op jit(solution)/shard_map/all_gather | solution.py:15
  15.5 257.0 %all-gather.6.cloned.1.call-start = ((), (), s32[]{:S(2)}) async-start(), calls=%async_computation.3 | async-start | bytes 3538944 | tf_op jit(solution)/shard_map/all_gather | solution.py:132
  159.9 46.4 %copy-start.4 = (bf16[96,2048]{1,0:T(8,128)(2,1)S(1)}, bf16[96,2048]{1,0:T(8,128)(2,1)}, u32[]{:S(2)}) copy-start(bf16[96,2048]{1,0:T(8,128)(2,1)} %param.19) | copy-start | bytes 1179652
  159.9 46.4 %copy-start.7 = (f32[2048]{0:T(1024)S(1)}, f32[2048]{0:T(1024)}, u32[]{:S(2)}) copy-start(f32[2048]{0:T(1024)} %param.21) | copy-start | bytes 24580
  205.6 1.1 copy-start.8
  207.7 77.8 %copy-start.5 = (f32[3,704]{1,0:T(4,128)S(1)}, f32[3,704]{1,0:T(4,128)}, u32[]{:S(2)}) copy-start(f32[3,704]{1,0:T(4,128)} %param.26) | copy-start | bytes 25348
  207.7 77.8 %copy-start.6 = (f32[3,704]{1,0:T(4,128)S(1)}, f32[3,704]{1,0:T(4,128)}, u32[]{:S(2)}) copy-start(f32[3,704]{1,0:T(4,128)} %param.25) | copy-start | bytes 25348
  280.9 4.6 %collective-permute-start = (bf16[1,1408]{1,0:T(2,128)(2,1)S(1)}, bf16[1,1408]{1,0:T(2,128)(2,1)S(1)}, u32[]{:S(2)}, u32[]{:S(2)}) collective-permute-start(bf16[1,1408]{1,0:T(2,128)(2,1)S(1)} %get-tuple-element.10), channel_id=1, source_target_pairs={{0,8},{8,16},{16,24},{24,32},{32,40},{40,48},{48,56},{56,64},{64,7... | collective-permute-start | bytes 8456 | tf_op jit(solution)/shard_map/ppermute | solution.py:38
  284.1 4.4 %collective-permute-start.1 = (bf16[1,1408]{1,0:T(2,128)(2,1)S(1)}, bf16[1,1408]{1,0:T(2,128)(2,1)S(1)}, u32[]{:S(2)}, u32[]{:S(2)}) collective-permute-start(bf16[1,1408]{1,0:T(2,128)(2,1)S(1)} %get-tuple-element.11), channel_id=1, source_target_pairs={{8,0},{16,8},{24,16},{32,24},{40,32},{48,40},{56,48},{64,56},{72,6... | collective-permute-start | bytes 8456 | tf_op jit(solution)/shard_map/ppermute | solution.py:41
  295.3 43.4 %copy-start.1 = (bf16[128,2048]{1,0:T(8,128)(2,1)S(1)}, bf16[128,2048]{1,0:T(8,128)(2,1)}, u32[]{:S(2)}) copy-start(bf16[128,2048]{1,0:T(8,128)(2,1)} %param.20) | copy-start | bytes 1572868
Sparse Core Ops, SparseCore 0:
  13.5 95.9 all-gather.3
  111.3 118.8 all-gather.7
  232.0 40.3 all-gather.5
where the time goes:
time: 346 us; the launch traced here: 345 us
  waiting for transfers between devices  161 us (47%)
  blocking collectives  87.7 us (25%)
  matrix products  48.5 us (14%)
  other arithmetic  28.9 us (8%)
  between operations  13.4 us (4%)
  starting transfers between devices  4.63 us (1%)
    all_gather x2, waiting for transfers between devices, sent_together(): lax.all_gather(both, axis, axis=dim, tiled=True)  116 us
    all_to_all x2, blocking collectives, summed_on_arrival(): lax.all_to_all(tiles, axis, split_axis=0, concat_axis=0, tiled=True)  87.7 us
    all_gather x1, waiting for transfers between devices, body(): lax.all_gather(normed, 'tp', axis=0, tiled=True)  42.3 us
    dot_general x1, matrix products, body(): jnp.dot(block_rows, out_weight, preferred_element_type=jnp.float32)  18.7 us
    dot_general x1, matrix products, body(): lax.dot_general(query_rows, key_piece, (((1,), (1,)), ((), ())), preferre...  16.3 us
    reduce_sum x1, other arithmetic, body(): denom = jnp.sum(weights, axis=1, keepdims=True)  15.4 us
    dot_general x1, matrix products, body(): jnp.dot(lax.all_gather(normed, 'tp', axis=0, tiled=True), paired, preferr...  8.42 us
  transfers between devices with their start and end apart: 5, of which 4 were waited for; matrix products, arithmetic and copies ran while one was open for 16% of the time, Pallas kernels for 0%

commit v1 on v0

--- a/solution.py
+++ b/solution.py
@@ -8,6 +8,28 @@
 GRID_W = 64
 EPSILON = 1e-06
 THETA = 10000.0
+
+
+def laid_out(blocks, dim):
+    lengths = list(blocks.shape[1:])
+    lengths[dim] *= blocks.shape[0]
+    return jnp.moveaxis(blocks, 0, dim).reshape(lengths)
+
+
+def gather_around(shard, axis, dim):
+    length = lax.axis_size(axis)
+    pairs = [(i, (i + 1) % length) for i in range(length)]
+    back = [(b, a) for a, b in pairs]
+    lower, upper = ([], [])
+    for step in range(length - 1):
+        if step % 2 == 0:
+            lower.append(lax.ppermute(lower[-1] if lower else shard, axis, pairs))
+        else:
+            upper.append(lax.ppermute(upper[-1] if upper else shard, axis, back))
+    blocks = jnp.stack([*lower[::-1], shard, *upper])
+    shift = lax.axis_index(axis) - len(lower)
+    blocks = blocks[(jnp.arange(length) - shift) % length]
+    return laid_out(blocks, dim)
 
 
 def sent_together(arrays, axis, dim, along):
@@ -129,7 +151,7 @@
     normed = rms_rows(stream, ffn_gain).astype(jnp.bfloat16)
     paired = jnp.concatenate([gate_rows, value_rows], axis=1)
     upward = jnp.dot(
-        lax.all_gather(normed, "tp", axis=0, tiled=True), paired, preferred_element_type=jnp.float32
+        gather_around(normed, "tp", 0), paired, preferred_element_type=jnp.float32
     ).astype(jnp.bfloat16)
     padded = with_halo(upward, (("sp", 0),), 1).astype(jnp.float32)
     taps = jnp.concatenate([conv_gate, conv_value], axis=1)

time: 346 us -> 324 us (0.936)
  waiting for transfers between devices: 161 us -> 110 us
  starting transfers between devices: 4.63 us -> 17.6 us
  local copies, waits for them, and re-layouts: 1.02 us -> 10.1 us
  blocking collectives: 87.7 us -> 93.9 us
    all_gather x1 -> x0, waiting for transfers between devices: 42.3 us -> none  [body(): lax.all_gather(normed, 'tp', axis=0, tiled=True)]
    all_gather x2, waiting for transfers between devices: 116 us -> 93.3 us  [sent_together(): lax.all_gather(both, axis, axis=dim, tiled=True)]
    ppermute x0 -> x7, waiting for transfers between devices: none -> 14 us  [the longest x4 13 us: gather_around(): lower.append(lax.ppermute(lower[-1] if lower else shard, axis, pairs))]
    ppermute x0 -> x7, starting transfers between devices: none -> 13.9 us  [the longest x4 9.02 us: gather_around(): lower.append(lax.ppermute(lower[-1] if lower else shard, axis, pairs))]
    all_to_all x2, blocking collectives: 87.7 us -> 93.9 us  [summed_on_arrival(): lax.all_to_all(tiles, axis, split_axis=0, concat_axis=0, tiled=True)]
    unnamed x22 -> x30, local copies, waits for them, and re-layouts: 0.05 us -> 5.02 us
    gather x0 -> x1, local copies, waits for them, and re-layouts: none -> 4.29 us  [gather_around(): blocks = blocks[(jnp.arange(length) - shift) % length]]
  transfers between devices with their start and end apart: 5 -> 11, of which waited for: 4 -> 8; matrix products, arithmetic and copies ran while one was open for 16% -> 20% of each run, Pallas kernels for 0% -> 0%
where the time goes in v1:
time: 324 us; the launch traced here: 323 us
  waiting for transfers between devices  110 us (34%)
  blocking collectives  93.9 us (29%)
  matrix products  48.5 us (15%)
  other arithmetic  29.1 us (9%)
  starting transfers between devices  17.6 us (5%)
  between operations  13.7 us (4%)
  local copies, waits for them, and re-layouts  10.1 us (3%)
    all_to_all x2, blocking collectives, summed_on_arrival(): lax.all_to_all(tiles, axis, split_axis=0, concat_axis=0, tiled=True)  93.9 us
    all_gather x2, waiting for transfers between devices, sent_together(): lax.all_gather(both, axis, axis=dim, tiled=True)  93.3 us
    dot_general x1, matrix products, body(): jnp.dot(block_rows, out_weight, preferred_element_type=jnp.float32)  18.7 us
    dot_general x1, matrix products, body(): lax.dot_general(query_rows, key_piece, (((1,), (1,)), ((), ())), preferre...  16.3 us
    reduce_sum x1, other arithmetic, body(): denom = jnp.sum(weights, axis=1, keepdims=True)  15.4 us
    ppermute x4, waiting for transfers between devices, gather_around(): lower.append(lax.ppermute(lower[-1] if lower else shard, axis, pairs))  13 us
    ppermute x4, starting transfers between devices, gather_around(): lower.append(lax.ppermute(lower[-1] if lower else shard, axis, pairs))  9.02 us
    dot_general x1, matrix products, body(): jnp.dot(gather_around(normed, 'tp', 0), paired, preferred_element_type=jn...  8.44 us
  transfers between devices with their start and end apart: 11, of which 8 were waited for; matrix products, arithmetic and copies ran while one was open for 20% of the time, Pallas kernels for 0%

profile of v1, /device:TPU:33, one launch (start us, length us, event | category | flops | bytes accessed | tf_op | source)
XLA Modules:
  0.0 323.3 jit_solution(18131975368113705969)
XLA Ops:
  6.5 0.0 copy-start
  6.6 0.1 all-gather.3.cloned.1.call-start
  6.7 1.2 fusion.55
  7.9 1.1 fusion.56
  9.0 0.4 slice_negate_fusion.1
  9.4 0.0 copy-start.2
  9.4 0.0 copy-start.10
  9.5 0.3 broadcast_multiply_fusion.1
  9.7 0.0 copy-done.3
  9.7 2.0 fusion.60
  11.7 0.8 pad_maximum_fusion.2
  12.5 0.1 all-gather.3.cloned.1.call-update
  12.6 0.1 all-gather.5.cloned.1.call-start
  12.7 1.9 pad_maximum_fusion
  14.6 0.1 all-gather.5.cloned.1.call-update
  14.6 0.2 fusion.48
  14.9 0.2 fusion.50
  15.0 0.4 fusion.58
  15.4 93.3 %all-gather.3.cloned.1.call-done = bf16[12288,256]{1,0:T(8,128)(2,1)} async-done(((bf16[768,256]{1,0:T(8,128)(2,1)}), bf16[12288,256]{1,0:T(8,128)(2,1)}) %all-gather.3.cloned.1.call-update) | async-done | bytes 6291472 | tf_op jit(solution)/shard_map/all_gather | solution.py:37
  108.7 16.3 %fusion.89 = (f32[768]{0:T(1024)S(1)}, f32[768,12288]{1,0:T(8,128)}) fusion(bf16[12288,256]{1,0:T(8,128)(2,1)} %all-gather.3.cloned.1.call-done, bf16[768,128]{1,0:T(8,128)(2,1)S(1)} %copy-done.2, f32[768,32]{1,0:T(8,128)S(1)} %get-tuple-element.13, f32[768,32]{1,0:T(8,128)S(1)} %get-tuple-element.14, f32[768,32]{1,0:T(8,128)S(1)} %get-tuple-element.15, ...), kind=kOutput, calls=%fused_computation.133 | convolution fusion | flops 2426731776 | bytes 41687552 | tf_op jit(solution)/shard_map/dot_general | solution.py:134
  125.0 15.4 %fusion = f32[768]{0:T(1024)S(1)} fusion(f32[768,12288]{1,0:T(8,128)} %get-tuple-element.23, f32[768]{0:T(1024)S(1)} %broadcast_maximum_fusion), kind=kLoop, calls=%fused_computation.2 | loop fusion | flops 18873600 | bytes 37754880 | tf_op jit(solution)/shard_map/reduce_sum | solution.py:139
  140.4 18.7 %convolution_convert_fusion.1 = bf16[768,2048]{1,0:T(8,128)(2,1)} fusion(bf16[128,2048]{1,0:T(8,128)(2,1)S(1)} %copy-done, bf16[12288,256]{1,0:T(8,128)(2,1)} %all-gather.3.cloned.1.call-done, f32[768,12288]{1,0:T(8,128)} %get-tuple-element.23, f32[768]{0:T(1024)S(1)} %broadcast_maximum_fusion, f32[768]{0:T(1024)S(1)} %fusion), kind=kOutput, calls=%fused_computation.17 | convolution fusion | flops 2839216128 | bytes 44570624 | tf_op jit(solution)/shard_map/dot_general | solution.py:146
  159.1 45.6 %all_to_all.10 = bf16[8,96,2048]{2,1,0:T(8,128)(2,1)S(1)} all-to-all(bf16[8,96,2048]{2,1,0:T(8,128)(2,1)} %bitcast.33), channel_id=1, replica_groups=mesh['grp'=2,'sp'=16,'tp'=8] {'tp'}, dimensions={0} | all-to-all | bytes 6291456 | tf_op jit(solution)/shard_map/all_to_all | solution.py:51
  204.7 0.6 convert_reduce_fusion.1
  205.2 0.1 multiply_reduce_fusion
  205.4 0.3 copy-done.4
  205.6 0.3 fusion.44
  206.0 0.2 fusion.46
  206.2 1.6 collective-permute-start
  207.7 4.7 %collective-permute-done = bf16[96,2048]{1,0:T(8,128)(2,1)S(1)} collective-permute-done((bf16[96,2048]{1,0:T(8,128)(2,1)S(1)}, bf16[96,2048]{1,0:T(8,128)(2,1)S(1)}, u32[]{:S(2)}, u32[]{:S(2)}) %collective-permute-start) | collective-permute-done | bytes 393248 | tf_op jit(solution)/shard_map/ppermute | solution.py:26
  212.5 2.5 collective-permute-start.1
  214.9 0.7 collective-permute-start.4
  215.6 4.1 %collective-permute-done.1 = bf16[96,2048]{1,0:T(8,128)(2,1)S(1)} collective-permute-done((bf16[96,2048]{1,0:T(8,128)(2,1)S(1)}, bf16[96,2048]{1,0:T(8,128)(2,1)S(1)}, u32[]{:S(2)}, u32[]{:S(2)}) %collective-permute-start.1) | collective-permute-done | bytes 393248 | tf_op jit(solution)/shard_map/ppermute | solution.py:26
  219.7 2.5 collective-permute-start.2
  222.2 0.3 collective-permute-done.4
  222.4 1.6 collective-permute-start.5
  224.0 2.8 collective-permute-done.2
  226.9 2.5 collective-permute-start.3
  229.4 0.7 collective-permute-done.5
  230.0 2.6 collective-permute-start.6
  232.7 1.4 collective-permute-done.3
  234.1 0.8 bitcast_dynamic-update-slice_fusion.7
  234.8 0.8 bitcast_dynamic-update-slice_fusion.6
  235.6 0.8 bitcast_dynamic-update-slice_fusion.5
  236.4 0.8 bitcast_dynamic-update-slice_fusion.4
  237.2 0.9 bitcast_dynamic-update-slice_fusion.3
  238.1 0.8 bitcast_dynamic-update-slice_fusion.2
  238.9 0.8 bitcast_dynamic-update-slice_fusion.1
  239.7 0.0 collective-permute-done.6
  239.7 0.8 bitcast_dynamic-update-slice_fusion
  240.5 4.3 %gather_fusion = bf16[8,96,2048]{2,1,0:T(8,128)(2,1)} fusion(bf16[8,96,2048]{2,1,0:T(8,128)(2,1)} %bitcast_dynamic-update-slice_fusion, s32[1024]{0:T(1024)S(1)} %pad_clamp_fusion), kind=kCustom, calls=%fused_computation | custom fusion | bytes 6291488 | tf_op jit(solution)/shard_map/gather | solution.py:31
  244.8 8.4 %fusion.9 = bf16[768,1408]{1,0:T(8,128)(2,1)S(1)} fusion(bf16[768,2048]{1,0:T(8,128)(2,1)} %bitcast.34, bf16[2048,2112]{0,1:T(8,128)(2,1)} %all-gather.5.cloned.1.call-done), kind=kOutput, calls=%fused_computation.18 | convolution fusion | flops 4430266368 | bytes 11075584 | tf_op jit(solution)/shard_map/dot_general | solution.py:153
  253.2 2.3 collective-permute-start.7
  255.5 1.3 collective-permute-start.8
  256.9 0.1 maximum_reduce_fusion.1
  257.0 0.0 collective-permute-done.7
  257.0 2.9 collective-permute-done.8
  259.9 0.4 maximum_convert_fusion
  260.4 1.3 fusion.7
  261.6 5.1 %convolution_convert_fusion = bf16[768,2048]{1,0:T(8,128)(2,1)S(1)} fusion(bf16[2048,2112]{0,1:T(8,128)(2,1)} %all-gather.5.cloned.1.call-done, f32[768,1408]{1,0:T(8,128)S(1)} %fusion.7), kind=kOutput, calls=%fused_computation.16 | convolution fusion | flops 2221572096 | bytes 10747904 | tf_op jit(solution)/shard_map/dot_general | solution.py:165
  266.8 0.0 copy-start.1
  266.8 48.3 %all_to_all.11 = bf16[8,96,2048]{2,1,0:T(8,128)(2,1)S(1)} all-to-all(bf16[8,96,2048]{2,1,0:T(8,128)(2,1)S(1)} %bitcast.35), channel_id=1, replica_groups=mesh['grp'=2,'sp'=16,'tp'=8] {'tp'}, dimensions={0} | all-to-all | bytes 6291456 | tf_op jit(solution)/shard_map/all_to_all | solution.py:51
  315.1 0.6 convert_reduce_fusion
  315.6 0.8 fusion.47
  (30 shorter events, 0.2 us)
Async XLA Ops:
  6.5 133.8 %copy-start = (bf16[128,2048]{1,0:T(8,128)(2,1)S(1)}, bf16[128,2048]{1,0:T(8,128)(2,1)}, u32[]{:S(2)}) copy-start(bf16[128,2048]{1,0:T(8,128)(2,1)} %param.20) | copy-start | bytes 1572868
  6.6 3.2 copy-start.3
  6.6 3.2 copy-start.11
  6.6 2.8 copy-start.5
  6.6 102.1 %all-gather.3.cloned.1.call-start = ((), (), s32[]{:S(2)}) async-start(), calls=%async_computation.2 | async-start | bytes 6684672 | tf_op jit(solution)/shard_map/all_gather | solution.py:37
  9.4 5.2 %copy-start.2 = (bf16[768,128]{1,0:T(8,128)(2,1)S(1)}, bf16[768,128]{1,0:T(8,128)(2,1)}, u32[]{:S(2)}) copy-start(bf16[768,128]{1,0:T(8,128)(2,1)} %param.14) | copy-start | bytes 589828
  9.4 5.4 %copy-start.10 = (f32[128]{0:T(128)S(1)}, f32[128]{0:T(128)}, u32[]{:S(2)}) copy-start(f32[128]{0:T(128)} %param.17) | copy-start | bytes 1540
  12.6 232.2 %all-gather.5.cloned.1.call-start = ((), (), s32[]{:S(2)}) async-start(), calls=%async_computation.3 | async-start | bytes 9191424 | tf_op jit(solution)/shard_map/all_gather | solution.py:37
  204.6 1.0 copy-start.4
  204.6 1.0 copy-start.9
  204.6 1.3 copy-start.6
  206.2 6.3 %collective-permute-start = (bf16[96,2048]{1,0:T(8,128)(2,1)S(1)}, bf16[96,2048]{1,0:T(8,128)(2,1)S(1)}, u32[]{:S(2)}, u32[]{:S(2)}) collective-permute-start(bf16[96,2048]{1,0:T(8,128)(2,1)S(1)} %fusion.46), channel_id=1, source_target_pairs={{0,1},{1,2},{2,3},{3,4},{4,5},{5,6},{6,7},{7,0},{8,9},{9,10},{10,1... | collective-permute-start | bytes 1179656 | tf_op jit(solution)/shard_map/ppermute | solution.py:26
  212.5 7.2 %collective-permute-start.1 = (bf16[96,2048]{1,0:T(8,128)(2,1)S(1)}, bf16[96,2048]{1,0:T(8,128)(2,1)S(1)}, u32[]{:S(2)}, u32[]{:S(2)}) collective-permute-start(bf16[96,2048]{1,0:T(8,128)(2,1)S(1)} %collective-permute-done), channel_id=1, source_target_pairs={{0,1},{1,2},{2,3},{3,4},{4,5},{5,6},{6,7},{7,0},{8,9},{9,10},{10,1... | collective-permute-start | bytes 1179656 | tf_op jit(solution)/shard_map/ppermute | solution.py:26
  214.9 7.5 %collective-permute-start.4 = (bf16[96,2048]{1,0:T(8,128)(2,1)S(1)}, bf16[96,2048]{1,0:T(8,128)(2,1)S(1)}, u32[]{:S(2)}, u32[]{:S(2)}) collective-permute-start(bf16[96,2048]{1,0:T(8,128)(2,1)S(1)} %fusion.46), channel_id=1, source_target_pairs={{1,0},{2,1},{3,2},{4,3},{5,4},{6,5},{7,6},{0,7},{9,8},{10,9},{11,1... | collective-permute-start | bytes 1179656 | tf_op jit(solution)/shard_map/ppermute | solution.py:28
  219.7 7.2 %collective-permute-start.2 = (bf16[96,2048]{1,0:T(8,128)(2,1)S(1)}, bf16[96,2048]{1,0:T(8,128)(2,1)S(1)}, u32[]{:S(2)}, u32[]{:S(2)}) collective-permute-start(bf16[96,2048]{1,0:T(8,128)(2,1)S(1)} %collective-permute-done.1), channel_id=1, source_target_pairs={{0,1},{1,2},{2,3},{3,4},{4,5},{5,6},{6,7},{7,0},{8,9},{9,10},{10,1... | collective-permute-start | bytes 1179656 | tf_op jit(solution)/shard_map/ppermute | solution.py:26
  222.4 7.6 %collective-permute-start.5 = (bf16[96,2048]{1,0:T(8,128)(2,1)S(1)}, bf16[96,2048]{1,0:T(8,128)(2,1)S(1)}, u32[]{:S(2)}, u32[]{:S(2)}) collective-permute-start(bf16[96,2048]{1,0:T(8,128)(2,1)S(1)} %collective-permute-done.4), channel_id=1, source_target_pairs={{1,0},{2,1},{3,2},{4,3},{5,4},{6,5},{7,6},{0,7},{9,8},{10,9},{11,1... | collective-permute-start | bytes 1179656 | tf_op jit(solution)/shard_map/ppermute | solution.py:28
  226.9 7.2 %collective-permute-start.3 = (bf16[96,2048]{1,0:T(8,128)(2,1)S(1)}, bf16[96,2048]{1,0:T(8,128)(2,1)S(1)}, u32[]{:S(2)}, u32[]{:S(2)}) collective-permute-start(bf16[96,2048]{1,0:T(8,128)(2,1)S(1)} %collective-permute-done.2), channel_id=1, source_target_pairs={{0,1},{1,2},{2,3},{3,4},{4,5},{5,6},{6,7},{7,0},{8,9},{9,10},{10,1... | collective-permute-start | bytes 1179656 | tf_op jit(solution)/shard_map/ppermute | solution.py:26
  230.0 9.6 %collective-permute-start.6 = (bf16[96,2048]{1,0:T(8,128)(2,1)S(1)}, bf16[96,2048]{1,0:T(8,128)(2,1)S(1)}, u32[]{:S(2)}, u32[]{:S(2)}) collective-permute-start(bf16[96,2048]{1,0:T(8,128)(2,1)S(1)} %collective-permute-done.5), channel_id=1, source_target_pairs={{1,0},{2,1},{3,2},{4,3},{5,4},{6,5},{7,6},{0,7},{9,8},{10,9},{11,1... | collective-permute-start | bytes 1179656 | tf_op jit(solution)/shard_map/ppermute | solution.py:28
  244.8 12.1 %copy-start.7 = (f32[3,704]{1,0:T(4,128)S(1)}, f32[3,704]{1,0:T(4,128)}, u32[]{:S(2)}) copy-start(f32[3,704]{1,0:T(4,128)} %param.26) | copy-start | bytes 25348
  244.8 12.1 %copy-start.8 = (f32[3,704]{1,0:T(4,128)S(1)}, f32[3,704]{1,0:T(4,128)}, u32[]{:S(2)}) copy-start(f32[3,704]{1,0:T(4,128)} %param.25) | copy-start | bytes 25348
  253.2 3.7 %collective-permute-start.7 = (bf16[1,1408]{1,0:T(2,128)(2,1)S(1)}, bf16[1,1408]{1,0:T(2,128)(2,1)S(1)}, u32[]{:S(2)}, u32[]{:S(2)}) collective-permute-start(bf16[1,1408]{1,0:T(2,128)(2,1)S(1)} %get-tuple-element.10), channel_id=1, source_target_pairs={{0,8},{8,16},{16,24},{24,32},{32,40},{40,48},{48,56},{56,64},{64,7... | collective-permute-start | bytes 8456 | tf_op jit(solution)/shard_map/ppermute | solution.py:60
  255.5 4.4 %collective-permute-start.8 = (bf16[1,1408]{1,0:T(2,128)(2,1)S(1)}, bf16[1,1408]{1,0:T(2,128)(2,1)S(1)}, u32[]{:S(2)}, u32[]{:S(2)}) collective-permute-start(bf16[1,1408]{1,0:T(2,128)(2,1)S(1)} %get-tuple-element.11), channel_id=1, source_target_pairs={{8,0},{16,8},{24,16},{32,24},{40,32},{48,40},{56,48},{64,56},{72,6... | collective-permute-start | bytes 8456 | tf_op jit(solution)/shard_map/ppermute | solution.py:63
  266.8 49.7 %copy-start.1 = (bf16[128,2048]{1,0:T(8,128)(2,1)S(1)}, bf16[128,2048]{1,0:T(8,128)(2,1)}, u32[]{:S(2)}) copy-start(bf16[128,2048]{1,0:T(8,128)(2,1)} %param.20) | copy-start | bytes 1572868
Sparse Core Ops, SparseCore 0:
  12.7 95.9 all-gather.2
  110.4 118.9 all-gather.4
